TPU v7x, 128 devices: a whole 4x4x4 slice. The times are simulated.
128 devices in a mesh: sp: 32 (over z, y, core), tp: 4 (over x).
Axes of the slice: x: 4, y: 4, z: 4, core: 2. Of those that a mesh axis runs over, the one named last changes fastest.
Arguments:
- queries: bfloat16 [6144, 1024], P('sp', 'tp'), may hold values from -0.75 to 0.75
- key_vectors: bfloat16 [6144, 1024], P('sp', 'tp'), may hold values from -0.75 to 0.75
- values_in: bfloat16 [6144, 2048], P('sp', 'tp'), may hold values from -0.75 to 0.75
- log_decay: float32 [6144, 1024], P('sp', 'tp'), may hold values from -1 to 0
- mixed_heads: bfloat16 [6144, 2048], P('sp', 'tp'), may hold values from -6 to 6
- out_proj: bfloat16 [2048, 2048], P('tp'), may hold values from -0.125 to 0.125
- layer_input: bfloat16 [6144, 2048], P('sp'), may hold values from -6 to 6
- cotangent: bfloat16 [6144, 2048], P('sp'), may hold values from -6 to 6
- routes: int32 [6144, 2], P('sp'), may hold values from 0 to 63, all different within a row; in each aligned block of 192 rows (0 to 191, 192 to 383, ...) at most 12 rows name the same one
- route_weight: float32 [6144, 2], P('sp'), may hold values from 0.25 to 2
- gate_weight: bfloat16 [64, 2048, 1024], P('sp', None, 'tp'), may hold values from -0.125 to 0.125
- up_weight: bfloat16 [64, 2048, 1024], P('sp', None, 'tp'), may hold values from -0.125 to 0.125
- down_weight: bfloat16 [64, 1024, 2048], P('sp', 'tp'), may hold values from -0.1875 to 0.1875
Outputs:
- grad_gate: float32 [64, 2048, 1024], P('sp', None, 'tp')
- grad_up: float32 [64, 2048, 1024], P('sp', None, 'tp')
- grad_down: float32 [64, 1024, 2048], P('sp', 'tp')
- grad_proj: float32 [2048, 2048], P('sp', 'tp')
- grad_query: float32 [6144, 1024], P('sp', 'tp')
- grad_key: float32 [6144, 1024], P('sp', 'tp')
- grad_value: float32 [6144, 2048], P('sp', 'tp')
- grad_decay: float32 [6144, 1024], P('sp', 'tp')
Inputs may be any that keep to these rules, and one draw needn't show every extreme that they name: `routes`: in each aligned block of 192 tokens no expert is named by more than 12 pairs, and in some block one expert is named by exactly 12 pairs; the 2 experts of a token differ.
All inputs are finite; a program needn't handle non-finite values.
Results may differ from a plain program's by a relative error of at most 0.015.
Values may be sent and summed in bfloat16 or wider, within the bound.
A program may use at most 192 MiB of HBM per device.

v0:
```python
import functools
import jax
import jax.numpy as jnp
from jax import lax
from jax.experimental import pallas as pl
from jax.experimental.pallas import tpu as pltpu
from jax.sharding import PartitionSpec as P

DK = 128
DV = 256
TOK = 192
SP = 32
TP = 4
CAP = 12
QW = 512
F32 = jnp.float32
BF16 = jnp.bfloat16
VM = pltpu.VMEM
CHIP_OFF = (
    (1, 0), (0, 1), (3, 0), (0, 3), (1, 1), (3, 3), (2, 0), (0, 2),
    (1, 3), (3, 1), (2, 1), (1, 2), (2, 3), (3, 2), (2, 2),
)
OFFS = ((0, 0, 1),) + tuple((dy, dz, dc) for dy, dz in CHIP_OFF for dc in (0, 1))


def moved(me, off, sign):
    dy, dz, dc = off
    core, y, z = lax.rem(me, 2), lax.rem(me // 2, 4), me // 8
    if sign < 0:
        dy, dz = (4 - dy) % 4, (4 - dz) % 4
    core = core if dc == 0 else 1 - core
    y = y if dy == 0 else lax.rem(y + dy, 4)
    z = z if dz == 0 else lax.rem(z + dz, 4)
    return (z * 4 + y) * 2 + core


def dot(a, b, dims, precision=None):
    return lax.dot_general(a, b, (dims, ((), ())), preferred_element_type=F32, precision=precision)


NN = ((1,), (0,))
NT = ((1,), (1,))
TN = ((0,), (0,))


def prep_kernel(routes_ref, weight_ref, rows_ref, cot_ref, place_ref, send_ref):
    mx = lax.axis_index("tp")
    experts = 2 * SP
    e_row = lax.broadcasted_iota(jnp.int32, (experts, TOK), 0)
    r0 = routes_ref[0:1, :]
    r1 = routes_ref[1:2, :]
    oh0 = jnp.where(e_row == r0, 1.0, 0.0)
    oh1 = jnp.where(e_row == r1, 1.0, 0.0)
    before = jnp.where(
        lax.broadcasted_iota(jnp.int32, (TOK, TOK), 0)
        < lax.broadcasted_iota(jnp.int32, (TOK, TOK), 1), 1.0, 0.0,
    )
    earlier = dot((oh0 + oh1).astype(BF16), before.astype(BF16), NN)
    slots = []
    for route, oh in ((r0, oh0), (r1, oh1)):
        rank = jnp.sum(oh * earlier, axis=0, keepdims=True).astype(jnp.int32)
        dest, local = route >> 1, route & 1
        pos = jnp.where(local == 0, rank, jnp.where(rank < 8, 16 + rank, 4 + rank))
        slots.append((pos >> 3) * (SP * 8) + dest * 8 + (pos & 7))
    slot_row = lax.broadcasted_iota(jnp.int32, (24 * SP, TOK), 0)
    hit0, hit1 = slot_row == slots[0], slot_row == slots[1]
    place = jnp.where(hit0 | hit1, 1.0, 0.0).astype(BF16)
    place_ref[...] = place
    weight = jnp.sum(
        jnp.where(hit0, weight_ref[0:1, :], 0.0) + jnp.where(hit1, weight_ref[1:2, :], 0.0),
        axis=1, keepdims=True,
    )
    for half in range(2):
        quarter = lax.rem(mx + 2 * half, TP)
        cols = pl.ds(pl.multiple_of(quarter * QW, QW), QW)
        send_ref[half, 0] = dot(place, rows_ref[:, cols], NN).astype(BF16)
        send_ref[half, 1] = (dot(place, cot_ref[:, cols], NN) * weight).astype(BF16)


def prep(routes_t, weight_t, rows, cot):
    return pl.pallas_call(
        prep_kernel,
        name="prep",
        out_shape=(
            jax.ShapeDtypeStruct((24 * SP, TOK), BF16),
            jax.ShapeDtypeStruct((2, 2, 24 * SP, QW), BF16),
        ),
        in_specs=[pl.BlockSpec(memory_space=VM)] * 4,
        out_specs=(pl.BlockSpec(memory_space=VM),) * 2,
        compiler_params=pltpu.CompilerParams(vmem_limit_bytes=32 << 20),
    )(routes_t, weight_t, rows, cot)


def dispatch_kernel(send_ref, out_ref, ssem, rsem, fsem, gsem, lsem):
    me, mx = lax.axis_index("sp"), lax.axis_index("tp")
    quarters = (mx, lax.rem(mx + 2, TP))
    sides = (lax.rem(mx + 1, TP), lax.rem(mx + 3, TP))
    barrier = pltpu.get_barrier_semaphore()
    for off in OFFS:
        pl.semaphore_signal(barrier, inc=1, device_id={"sp": moved(me, off, 1)})
    for side in sides:
        pl.semaphore_signal(barrier, inc=1, device_id={"tp": side})
    pl.semaphore_wait(barrier, len(OFFS) + 2)

    def plane(half, i):
        peer = moved(me, OFFS[i], 1)
        return pltpu.make_async_remote_copy(
            src_ref=send_ref.at[half, :, :, peer],
            dst_ref=out_ref.at[:, quarters[half], :, me],
            send_sem=ssem.at[half, i], recv_sem=rsem.at[half, i], device_id={"sp": peer},
        )

    def forward(way, i, src):
        return pltpu.make_async_remote_copy(
            src_ref=out_ref.at[:, quarters[0], :, src],
            dst_ref=out_ref.at[:, quarters[0], :, src],
            send_sem=fsem.at[way, i], recv_sem=gsem.at[way, i], device_id={"tp": sides[way]},
        )

    own = [
        pltpu.make_async_copy(
            send_ref.at[half, :, :, me], out_ref.at[:, quarters[half], :, me], lsem.at[half]
        )
        for half in range(2)
    ]
    for half in range(2):
        own[half].start()
    for half in range(2):
        for i in range(len(OFFS)):
            plane(half, i).start()
    own[0].wait()
    for way in range(2):
        forward(way, len(OFFS), me).start()
    for i, off in enumerate(OFFS):
        plane(0, i).wait_recv()
        for way in range(2):
            forward(way, i, moved(me, off, -1)).start()
    own[1].wait()
    for i in range(len(OFFS)):
        plane(1, i).wait_recv()
    for i in range(len(OFFS)):
        plane(0, i).wait_send()
        plane(1, i).wait_send()
    for i in range(len(OFFS) + 1):
        src = me if i == len(OFFS) else moved(me, OFFS[i], -1)
        for way in range(2):
            forward(way, i, src).wait()


def dispatch(send):
    n = len(OFFS)
    return pl.pallas_call(
        dispatch_kernel,
        name="dispatch",
        out_shape=jax.ShapeDtypeStruct((2, TP, 3, SP, 8, QW), BF16),
        in_specs=[pl.BlockSpec(memory_space=VM)],
        out_specs=pl.BlockSpec(memory_space=VM),
        scratch_shapes=[
            pltpu.SemaphoreType.DMA((2, n)),
            pltpu.SemaphoreType.DMA((2, n)),
            pltpu.SemaphoreType.DMA((2, n + 1)),
            pltpu.SemaphoreType.DMA((2, n + 1)),
            pltpu.SemaphoreType.DMA((2,)),
        ],
        compiler_params=pltpu.CompilerParams(
            collective_id=1, has_side_effects=True, vmem_limit_bytes=24 << 20
        ),
    )(send)


def expert_kernel(rows_ref, gate_ref, up_ref, down_ref, part_ref, act_ref, dg_ref, du_ref):
    for e in range(2):
        rows = pl.ds(256 * e, 512)
        pre_gate = pre_up = d_act = None
        for q in range(TP):
            cols = pl.ds(q * QW, QW)
            x, w = rows_ref[0, q, rows], rows_ref[1, q, rows]
            terms = (
                dot(x, gate_ref[e, cols], NN),
                dot(x, up_ref[e, cols], NN),
                dot(w, down_ref[e, :, cols], NT),
            )
            if q == 0:
                pre_gate, pre_up, d_act = terms
            else:
                pre_gate, pre_up, d_act = pre_gate + terms[0], pre_up + terms[1], d_act + terms[2]
        row = lax.broadcasted_iota(jnp.int32, (512, 256), 0)
        if e == 0:
            mine = (row < 256) | ((row & 7) < 4)
        else:
            mine = (row >= 256) | ((row & 7) >= 4)
        sig = jax.nn.sigmoid(pre_gate)
        silu = pre_gate * sig
        act_ref[e] = jnp.where(mine, silu * pre_up, 0.0).astype(BF16)
        dg = jnp.where(mine, d_act * pre_up * sig * (1.0 + pre_gate * (1.0 - sig)), 0.0).astype(BF16)
        du = jnp.where(mine, d_act * silu, 0.0).astype(BF16)
        dg_ref[e] = dg
        du_ref[e] = du
        for q in range(TP):
            cols = pl.ds(q * QW, QW)
            part = dot(dg, gate_ref[e, cols], NT) + dot(du, up_ref[e, cols], NT)
            if e == 0:
                part_ref[q, 0:512] = part.astype(BF16)
            else:
                part_ref[q, 256:512] = (part_ref[q, 256:512].astype(F32) + part[:256]).astype(BF16)
                part_ref[q, 512:768] = part[256:].astype(BF16)


def experts(rows, gate, up, down):
    hidden = jax.ShapeDtypeStruct((2, 512, 256), BF16)
    return pl.pallas_call(
        expert_kernel,
        name="experts",
        out_shape=(jax.ShapeDtypeStruct((TP, 24 * SP, QW), BF16), hidden, hidden, hidden),
        in_specs=[pl.BlockSpec(memory_space=VM)] * 4,
        out_specs=(pl.BlockSpec(memory_space=VM),) * 4,
        compiler_params=pltpu.CompilerParams(vmem_limit_bytes=48 << 20),
    )(rows, gate, up, down)


def weight_grad_kernel(rows_ref, act_ref, dg_ref, du_ref, gg_ref, gu_ref, gd_ref):
    rows = pl.ds(pl.multiple_of(pl.program_id(1) * 256, 256), 512)
    x, w = rows_ref[0, 0, rows], rows_ref[1, 0, rows]
    gg_ref[0] = dot(x, dg_ref[0], TN)
    gu_ref[0] = dot(x, du_ref[0], TN)
    gd_ref[0] = dot(act_ref[0], w, TN)


def weight_grads(rows, act, dg, du):
    hidden = pl.BlockSpec((1, 512, 256), lambda q, e: (e, 0, 0))
    wide = pl.BlockSpec((1, QW, 256), lambda q, e: (e, q, 0))
    return pl.pallas_call(
        weight_grad_kernel,
        name="weight_grads",
        grid=(TP, 2),
        out_shape=(
            jax.ShapeDtypeStruct((2, 2048, 256), F32),
            jax.ShapeDtypeStruct((2, 2048, 256), F32),
            jax.ShapeDtypeStruct((2, 256, 2048), F32),
        ),
        in_specs=[
            pl.BlockSpec((2, 1, 24 * SP, QW), lambda q, e: (0, q, 0, 0)), hidden, hidden, hidden,
        ],
        out_specs=(wide, wide, pl.BlockSpec((1, 256, QW), lambda q, e: (e, 0, q))),
        compiler_params=pltpu.CompilerParams(vmem_limit_bytes=48 << 20),
    )(rows, act, dg, du)


def heads(x, width):
    return x.reshape(x.shape[0], 2, width)


def exchange(x):
    return lax.all_to_all(x, "sp", split_axis=0, concat_axis=0, tiled=True)


def scan_states(decay, first, second, backward):
    n = first.shape[1] * 2 // SP
    both = jnp.stack([first, second], axis=0).reshape(2, SP, n, DK).transpose(1, 0, 2, 3)
    got = exchange(both.astype(BF16)).astype(F32)
    head = lax.axis_index("sp") // (SP // 2)
    d = lax.dynamic_index_in_dim(decay, head, 1, keepdims=False)
    acc = jnp.zeros_like(got[0])
    outs = [None] * SP
    for s in (range(SP - 1, -1, -1) if backward else range(SP)):
        outs[s] = acc
        acc = d[s][None, None, :] * acc + got[s]
    back = exchange(jnp.stack(outs).astype(BF16)).astype(F32)
    back = back.transpose(1, 0, 2, 3).reshape(2, 2, DV, DK)
    return back[0], back[1]


def body(
    queries, key_vectors, values_in, log_decay, mixed_heads, out_proj, layer_input, cotangent,
    routes, route_weight, gate_weight, up_weight, down_weight,
):
    mx = lax.axis_index("tp")
    place, send = prep(routes.T, route_weight.T, layer_input, cotangent)
    got = dispatch(send.reshape(2, 2, 3, SP, 8, QW)).reshape(2, TP, 24 * SP, QW)
    part, act, dg, du = experts(got, gate_weight, up_weight, down_weight)
    grad_gate, grad_up, grad_down = weight_grads(got, act, dg, du)
    mine = lax.psum_scatter(part, "tp", scatter_dimension=0, tiled=True)
    back = lax.all_to_all(
        mine.reshape(3, SP, 8, QW), "sp", split_axis=1, concat_axis=1, tiled=True
    ).reshape(24 * SP, QW)
    own_cot = lax.dynamic_slice_in_dim(cotangent, mx * QW, QW, 1)
    token_part = (own_cot.astype(F32) + dot(place, back, TN)).astype(BF16)
    token_grad = lax.all_gather(token_part, "tp", axis=1, tiled=True)
    grad_proj = lax.psum_scatter(
        dot(token_grad, mixed_heads, TN), "sp", scatter_dimension=0, tiled=True
    )
    sigma = DK ** (-0.5)
    grad_f = heads(dot(token_grad, out_proj, NT), DV)
    q, k, v = heads(queries, DK).astype(F32), heads(key_vectors, DK).astype(F32), heads(values_in, DV)
    t_row = lax.broadcasted_iota(jnp.int32, (TOK, TOK), 0)
    t_col = lax.broadcasted_iota(jnp.int32, (TOK, TOK), 1)
    lower = t_row >= t_col
    cum = heads(dot(lower.astype(F32), log_decay, NN, lax.Precision.HIGHEST), DK)
    total = cum[-1]
    rise, fall = jnp.exp(cum - 0.5 * total), jnp.exp(0.5 * total - cum)
    head, tail = jnp.exp(cum), jnp.exp(total - cum)
    decay = lax.all_gather(jnp.exp(total), "sp")

    def mm(eq, a, b):
        return jnp.einsum(eq, a.astype(BF16), b.astype(BF16), preferred_element_type=F32)

    qr, qf, kr, kf = q * rise, q * fall, k * rise, k * fall
    qh, qt, kh, kt = q * head, q * tail, k * head, k * tail
    score = sigma * (
        jnp.where(lower, mm("thc,shc->hts", qr, kf), 0.0) + jnp.where(lower, 0.0, mm("thc,shc->hts", qf, kr))
    )
    pair = mm("thv,shv->hts", grad_f, v)
    pair_fwd, pair_bwd = jnp.where(lower, pair, 0.0), jnp.where(lower, 0.0, pair)
    kv_fwd, kv_bwd = mm("shv,shc->hvc", v, kt), mm("shv,shc->hvc", v, kh)
    qo_bwd, qo_fwd = mm("thv,thc->hvc", grad_f, qt), mm("thv,thc->hvc", grad_f, qh)
    kv_low, qo_low = scan_states(decay, kv_fwd, qo_bwd, False)
    qo_high, kv_high = scan_states(decay, qo_fwd, kv_bwd, True)
    q_fwd = sigma * (rise * mm("hts,shc->thc", pair_fwd, kf) + head * mm("thv,hvc->thc", grad_f, kv_low))
    q_bwd = sigma * (fall * mm("hts,shc->thc", pair_bwd, kr) + tail * mm("thv,hvc->thc", grad_f, kv_high))
    k_fwd = sigma * (fall * mm("hts,thc->shc", pair_fwd, qr) + tail * mm("shv,hvc->shc", v, qo_high))
    k_bwd = sigma * (rise * mm("hts,thc->shc", pair_bwd, qf) + head * mm("shv,hvc->shc", v, qo_low))
    value_grad = mm("hts,thv->shv", score, grad_f) + sigma * (
        mm("shc,hvc->shv", kt, qo_high) + mm("shc,hvc->shv", kh, qo_low)
    )
    grad_cum = (q * (q_fwd - q_bwd) - k * (k_fwd - k_bwd)).reshape(TOK, 2 * DK)
    d_own = jnp.exp(total)[:, None, :]
    beyond = sigma * jnp.sum(
        (d_own * kv_low + kv_fwd) * qo_high + (d_own * qo_low + qo_bwd) * kv_high, axis=1
    ).reshape(1, 2 * DK)
    upper = (t_row <= t_col).astype(F32)
    grad_decay = dot(upper, grad_cum, NN, lax.Precision.HIGHEST) + beyond
    return (
        grad_gate, grad_up, grad_down, grad_proj,
        (q_fwd + q_bwd).reshape(TOK, 2 * DK), (k_fwd + k_bwd).reshape(TOK, 2 * DK),
        value_grad.reshape(TOK, 2 * DV), grad_decay,
    )


def solution(mesh):
    return jax.shard_map(
        body,
        mesh=mesh,
        in_specs=(
            P("sp", "tp"), P("sp", "tp"), P("sp", "tp"), P("sp", "tp"), P("sp", "tp"),
            P("tp", None), P("sp", None), P("sp", None), P("sp", None), P("sp", None),
            P("sp", None, "tp"), P("sp", None, "tp"), P("sp", "tp", None),
        ),
        out_specs=(
            P("sp", None, "tp"), P("sp", None, "tp"), P("sp", "tp", None),
            P("sp", "tp"), P("sp", "tp"), P("sp", "tp"), P("sp", "tp"), P("sp", "tp"),
        ),
        check_vma=False,
    )
```

profile of v0, /device:TPU:1, one launch (start us, length us, event | category | flops | bytes accessed | tf_op | source)
XLA Modules:
  0.0 295.4 jit_solution(3979245317002677246)
XLA Ops:
  12.3 49.3 %dispatch.1 = bf16[2,4,3,32,8,512]{5,4,3,2,1,0:T(8,128)(2,1)S(1)} custom-call(bf16[2,2,3,32,8,512]{5,4,3,2,1,0:T(8,128)(2,1)S(1)} %bitcast.388), custom_call_target="tpu_custom_call" | custom-call | tf_op jit(solution)/shard_map/dispatch/pallas_call | solution.py:152
  61.6 2.6 copy-done.1
  64.3 12.0 %experts.1 = (bf16[4,768,512]{2,1,0:T(8,128)(2,1)}, bf16[2,512,256]{2,1,0:T(8,128)(2,1)S(1)}, bf16[2,512,256]{2,1,0:T(8,128)(2,1)S(1)}, bf16[2,512,256]{2,1,0:T(8,128)(2,1)S(1)}) custom-call(bf16[2,4,768,512]{3,2,1,0:T(8,128)(2,1)} %bitcast.386, bf16[2,2048,256]{2,1,0:T(8,128)(2,1)S(1)} %copy-done.2, bf16[2,2048,256]{2,1,0:T(8,128)(2,1)S(1)} %copy-done.3, ...), custom_call_target="tpu_custom_call" | custom-call | tf_op jit(solution)/shard_map/experts/pallas_call | solution.py:211
  78.9 1.6 fusion.34
  81.2 1.8 fusion.22
  83.0 1.7 copy.151
  84.7 2.1 fusion.136
  86.7 1.7 copy.140
  89.4 12.7 %weight_grads.1 = (f32[2,2048,256]{2,1,0:T(8,128)}, f32[2,2048,256]{2,1,0:T(8,128)}, f32[2,256,2048]{2,1,0:T(8,128)}) custom-call(bf16[2,4,768,512]{3,2,1,0:T(8,128)(2,1)} %bitcast.387, bf16[2,512,256]{2,1,0:T(8,128)(2,1)S(1)} %get-tuple-element.18.act_ref, bf16[2,512,256]{2,1,0:T(8,128)(2,1)S(1)} %get-tuple-element.19.dg_ref, bf16[2,512,256]{2,1,0:T(8,128)(2,1)S(1)} %copy-done.7), custom_call_target="tpu_custom_call" | custom-call | tf_op jit(solution)/shard_map/weight_grads/pallas_call | solution.py:232
  102.1 24.8 %all_gather.8 = f32[32,2,128]{2,1,0:T(2,128)S(1)} all-gather(f32[1,2,128]{2,1,0:T(2,128)S(1)} %bitcast.426), channel_id=1, replica_groups=mesh['sp'=32,'tp'=4] {'sp'}, dimensions={0}, use_global_device_ids=true | all-gather | bytes 33792 | tf_op jit(solution)/shard_map/all_gather | solution.py:302
  127.5 2.1 copy.129
  129.6 4.3 %all-to-all-start = ((bf16[3,32,8,512]{3,2,0,1:T(8,128)(2,1)}), bf16[3,32,8,512]{3,2,0,1:T(8,128)(2,1)S(1)}, u32[]{:S(2)}, u32[]{:S(2)}) async-start(bf16[3,32,8,512]{3,2,0,1:T(8,128)(2,1)} %copy.129), calls=%async_computation.1 | async-start | bytes 1572864 | tf_op jit(solution)/shard_map/all_to_all | solution.py:283
  135.9 1.9 convolution_select_fusion
  137.8 10.3 %all-to-all-done = bf16[3,32,8,512]{3,2,0,1:T(8,128)(2,1)S(1)} async-done(((bf16[3,32,8,512]{3,2,0,1:T(8,128)(2,1)}), bf16[3,32,8,512]{3,2,0,1:T(8,128)(2,1)S(1)}, u32[]{:S(2)}, u32[]{:S(2)}) %all-to-all-start) | async-done | bytes 786464 | tf_op jit(solution)/shard_map/all_to_all | solution.py:283
  148.2 1.3 fusion.5
  149.6 12.3 %all_gather.7 = bf16[192,2048]{1,0:T(8,128)(2,1)S(1)} all-gather(bf16[192,512]{1,0:T(8,128)(2,1)S(1)} %fusion.5), channel_id=1, replica_groups=mesh['sp'=32,'tp'=4] {'tp'}, dimensions={1}, use_global_device_ids=true | all-gather | bytes 983040 | tf_op jit(solution)/shard_map/all_gather | solution.py:288
  166.9 6.4 %all-to-all-start.1 = ((bf16[32,2,16,128]{3,2,1,0:T(8,128)(2,1)}), bf16[32,2,16,128]{3,2,1,0:T(8,128)(2,1)}, u32[]{:S(2)}, u32[]{:S(2)}) async-start(bf16[32,2,16,128]{3,2,1,0:T(8,128)(2,1)} %copy.143), calls=%async_computation.3 | async-start | bytes 524288 | tf_op jit(solution)/shard_map/all_to_all | solution.py:254
  173.4 3.7 %fusion.141 = f32[2048,512]{1,0:T(8,128)} fusion(bf16[192,2048]{1,0:T(8,128)(2,1)S(1)} %all_gather.7, bf16[192,512]{1,0:T(8,128)(2,1)} %param.17), kind=kOutput, calls=%fused_computation.333 | convolution fusion | flops 402653184 | bytes 5177344 | tf_op jit(solution)/shard_map/dot_general | solution.py:38
  179.8 2.6 all-to-all-done.1
  182.4 5.0 %all-to-all-start.3 = ((bf16[32,2,16,128]{3,2,1,0:T(8,128)(2,1)}), bf16[32,2,16,128]{3,2,1,0:T(8,128)(2,1)S(1)}, u32[]{:S(2)}, u32[]{:S(2)}) async-start(bf16[32,2,16,128]{3,2,1,0:T(8,128)(2,1)} %copy.152), calls=%async_computation.5 | async-start | bytes 524288 | tf_op jit(solution)/shard_map/all_to_all | solution.py:254
  190.4 6.0 %all-to-all-done.3 = bf16[32,2,16,128]{3,2,1,0:T(8,128)(2,1)S(1)} async-done(((bf16[32,2,16,128]{3,2,1,0:T(8,128)(2,1)}), bf16[32,2,16,128]{3,2,1,0:T(8,128)(2,1)S(1)}, u32[]{:S(2)}, u32[]{:S(2)}) %all-to-all-start.3) | async-done | bytes 262176 | tf_op jit(solution)/shard_map/all_to_all | solution.py:254
  196.4 1.7 constant_dynamic-update-slice_fusion.63
  201.3 1.4 constant_dynamic-update-slice_fusion.25
  204.6 1.4 constant_dynamic-update-slice_fusion.23
  206.5 1.3 constant_dynamic-update-slice_fusion.22
  207.9 1.4 constant_dynamic-update-slice_fusion.21
  209.8 1.3 constant_dynamic-update-slice_fusion.20
  211.2 1.4 constant_dynamic-update-slice_fusion.19
  213.1 1.3 constant_dynamic-update-slice_fusion.18
  214.5 1.4 constant_dynamic-update-slice_fusion.17
  217.8 1.4 constant_dynamic-update-slice_fusion.15
  221.0 1.4 constant_dynamic-update-slice_fusion.13
  224.3 1.4 constant_dynamic-update-slice_fusion.11
  226.3 1.3 constant_dynamic-update-slice_fusion.10
  227.6 1.4 constant_dynamic-update-slice_fusion.9
  230.9 1.4 constant_dynamic-update-slice_fusion.7
  232.9 1.3 constant_dynamic-update-slice_fusion.6
  234.2 1.4 constant_dynamic-update-slice_fusion.5
  237.5 1.4 constant_dynamic-update-slice_fusion.3
  240.8 1.4 constant_dynamic-update-slice_fusion.1
  244.7 3.8 %all-to-all-start.4 = ((bf16[32,2,16,128]{3,2,1,0:T(8,128)(2,1)}), bf16[32,2,16,128]{3,2,1,0:T(8,128)(2,1)S(1)}, u32[]{:S(2)}, u32[]{:S(2)}) async-start(bf16[32,2,16,128]{3,2,1,0:T(8,128)(2,1)} %constant_dynamic-update-slice_fusion.32), calls=%async_computation.6 | async-start | bytes 524288 | tf_op jit(solution)/shard_map/all_to_all | solution.py:254
  248.4 1.9 fusion.19
  252.5 5.6 %all-to-all-done.4 = bf16[32,2,16,128]{3,2,1,0:T(8,128)(2,1)S(1)} async-done(((bf16[32,2,16,128]{3,2,1,0:T(8,128)(2,1)}), bf16[32,2,16,128]{3,2,1,0:T(8,128)(2,1)S(1)}, u32[]{:S(2)}, u32[]{:S(2)}) %all-to-all-start.4) | async-done | bytes 262176 | tf_op jit(solution)/shard_map/all_to_all | solution.py:254
  258.1 4.4 %all-to-all-start.2 = ((bf16[32,2,16,128]{3,2,1,0:T(8,128)(2,1)}), bf16[32,2,16,128]{3,2,1,0:T(8,128)(2,1)}, u32[]{:S(2)}, u32[]{:S(2)}) async-start(bf16[32,2,16,128]{3,2,1,0:T(8,128)(2,1)} %constant_dynamic-update-slice_fusion), calls=%async_computation.4 | async-start | bytes 524288 | tf_op jit(solution)/shard_map/all_to_all | solution.py:254
  264.2 7.2 %all-to-all-done.2 = bf16[32,2,16,128]{3,2,1,0:T(8,128)(2,1)} async-done(((bf16[32,2,16,128]{3,2,1,0:T(8,128)(2,1)}), bf16[32,2,16,128]{3,2,1,0:T(8,128)(2,1)}, u32[]{:S(2)}, u32[]{:S(2)}) %all-to-all-start.2) | async-done | bytes 262176 | tf_op jit(solution)/shard_map/all_to_all | solution.py:254
  276.1 2.4 fusion
  278.5 1.8 copy.184
  280.3 1.8 copy.169
  (169 shorter events, 59.7 us)
Async XLA Ops:
  7.2 154.7 %copy-start = (bf16[512,2048]{1,0:T(8,128)(2,1)S(1)}, bf16[512,2048]{1,0:T(8,128)(2,1)}, u32[]{:S(2)}) copy-start(bf16[512,2048]{1,0:T(8,128)(2,1)} %param.18) | copy-start | bytes 6291460
  7.2 120.3 %reduce-scatter.3.cloned.1.call-start = ((), (), s32[]{:S(2)}) async-start(), calls=%async_computation.7 | async-start | bytes 3932160 | tf_op jit(solution)/shard_map/reduce_scatter | solution.py:282
  7.2 1.3 copy-start.4
  8.5 1.1 copy-start.5
  12.3 52.0 %copy-start.2 = (bf16[2,2048,256]{2,1,0:T(8,128)(2,1)S(1)}, bf16[2,2048,256]{2,1,0:T(8,128)(2,1)}, u32[]{:S(2)}) copy-start(bf16[2,2048,256]{2,1,0:T(8,128)(2,1)} %gate_ref.1) | copy-start | bytes 6291460
  12.3 52.0 %copy-start.3 = (bf16[2,2048,256]{2,1,0:T(8,128)(2,1)S(1)}, bf16[2,2048,256]{2,1,0:T(8,128)(2,1)}, u32[]{:S(2)}) copy-start(bf16[2,2048,256]{2,1,0:T(8,128)(2,1)} %up_ref.1) | copy-start | bytes 6291460
  61.6 2.6 copy-start.1
  78.3 86.9 %copy-start.36 = (f32[1,256]{1,0:T(1,128)}, f32[1,256]{1,0:T(1,128)S(1)}, u32[]{:S(2)}) copy-start(f32[1,256]{1,0:T(1,128)S(1)} %get-tuple-element.82) | copy-start | bytes 3076
  102.1 33.7 %copy-start.11 = (f32[192,256]{1,0:T(8,128)S(1)}, f32[192,256]{1,0:T(8,128)}, u32[]{:S(2)}) copy-start(f32[192,256]{1,0:T(8,128)} %copy-done.10) | copy-start | bytes 589828
  129.6 18.5 %all-to-all-start = ((bf16[3,32,8,512]{3,2,0,1:T(8,128)(2,1)}), bf16[3,32,8,512]{3,2,0,1:T(8,128)(2,1)S(1)}, u32[]{:S(2)}, u32[]{:S(2)}) async-start(bf16[3,32,8,512]{3,2,0,1:T(8,128)(2,1)} %copy.129), calls=%async_computation.1 | async-start | bytes 1572864 | tf_op jit(solution)/shard_map/all_to_all | solution.py:283
  135.3 12.9 %copy-start.31 = (pred[192,192]{1,0:T(8,128)(4,1)}, pred[192,192]{1,0:T(8,128)(4,1)S(1)}, u32[]{:S(2)}) copy-start(pred[192,192]{1,0:T(8,128)(4,1)S(1)} %iota_compare_fusion.1) | copy-start | bytes 110596
  135.9 43.0 %copy-start.38 = (f32[2,128]{1,0:T(2,128)}, f32[2,128]{1,0:T(2,128)S(1)}, u32[]{:S(2)}) copy-start(f32[2,128]{1,0:T(2,128)S(1)} %get-tuple-element.116) | copy-start | bytes 3076
  148.2 14.6 %copy-start.16 = (bf16[192,256]{1,0:T(8,128)(2,1)S(1)}, bf16[192,256]{1,0:T(8,128)(2,1)}, u32[]{:S(2)}) copy-start(bf16[192,256]{1,0:T(8,128)(2,1)} %param.13) | copy-start | bytes 294916
  148.2 14.8 %copy-start.12 = (bf16[192,512]{1,0:T(8,128)(2,1)S(1)}, bf16[192,512]{1,0:T(8,128)(2,1)}, u32[]{:S(2)}) copy-start(bf16[192,512]{1,0:T(8,128)(2,1)} %param.15) | copy-start | bytes 589828
  149.5 13.7 %copy-start.32 = (pred[192,192]{1,0:T(8,128)(4,1)S(1)}, pred[192,192]{1,0:T(8,128)(4,1)}, u32[]{:S(2)}) copy-start(pred[192,192]{1,0:T(8,128)(4,1)} %copy-done.31) | copy-start | bytes 110596
  161.9 4.3 %copy-start.30 = (bf16[2,256,128]{2,1,0:T(8,128)(2,1)S(1)}, bf16[2,256,128]{2,1,0:T(8,128)(2,1)}, u32[]{:S(2)}) copy-start(bf16[2,256,128]{2,1,0:T(8,128)(2,1)} %copy.140) | copy-start | bytes 393220
  163.3 3.0 %copy-start.45 = (bf16[2,192,192]{2,1,0:T(8,128)(2,1)}, bf16[2,192,192]{2,1,0:T(8,128)(2,1)S(1)}, u32[]{:S(2)}) copy-start(bf16[2,192,192]{2,1,0:T(8,128)(2,1)S(1)} %fusion.39) | copy-start | bytes 442372
  166.9 15.5 %all-to-all-start.1 = ((bf16[32,2,16,128]{3,2,1,0:T(8,128)(2,1)}), bf16[32,2,16,128]{3,2,1,0:T(8,128)(2,1)}, u32[]{:S(2)}, u32[]{:S(2)}) async-start(bf16[32,2,16,128]{3,2,1,0:T(8,128)(2,1)} %copy.143), calls=%async_computation.3 | async-start | bytes 524288 | tf_op jit(solution)/shard_map/all_to_all | solution.py:254
  173.4 115.2 %reduce-scatter.5.cloned.1.call-start = ((), (), s32[]{:S(2)}) async-start(), calls=%async_computation.8 | async-start | bytes 4325376 | tf_op jit(solution)/shard_map/reduce_scatter | solution.py:289
  177.1 1.8 copy-start.20
  177.1 1.8 copy-start.33
  177.1 1.8 copy-start.46
  178.8 9.6 %copy-start.42 = (f32[128]{0:T(128)S(1)}, f32[128]{0:T(128)}, u32[]{:S(2)}) copy-start(f32[128]{0:T(128)} %get-tuple-element.100) | copy-start | bytes 1540
  178.9 10.3 %copy-start.43 = (f32[128]{0:T(128)S(1)}, f32[128]{0:T(128)}, u32[]{:S(2)}) copy-start(f32[128]{0:T(128)} %get-tuple-element.114) | copy-start | bytes 1540
  178.9 10.9 %copy-start.41 = (f32[128]{0:T(128)S(1)}, f32[128]{0:T(128)}, u32[]{:S(2)}) copy-start(f32[128]{0:T(128)} %get-tuple-element.113) | copy-start | bytes 1540
  178.9 17.6 %copy-start.39 = (f32[128]{0:T(128)S(1)}, f32[128]{0:T(128)}, u32[]{:S(2)}) copy-start(f32[128]{0:T(128)} %get-tuple-element.111) | copy-start | bytes 1540
  178.9 17.6 %copy-start.40 = (f32[128]{0:T(128)S(1)}, f32[128]{0:T(128)}, u32[]{:S(2)}) copy-start(f32[128]{0:T(128)} %get-tuple-element.86) | copy-start | bytes 1540
  179.8 68.6 %copy-start.34 = (pred[192,192]{1,0:T(8,128)(4,1)S(1)}, pred[192,192]{1,0:T(8,128)(4,1)}, u32[]{:S(2)}) copy-start(pred[192,192]{1,0:T(8,128)(4,1)} %copy-done.31) | copy-start | bytes 110596
  182.4 13.9 %all-to-all-start.3 = ((bf16[32,2,16,128]{3,2,1,0:T(8,128)(2,1)}), bf16[32,2,16,128]{3,2,1,0:T(8,128)(2,1)S(1)}, u32[]{:S(2)}, u32[]{:S(2)}) async-start(bf16[32,2,16,128]{3,2,1,0:T(8,128)(2,1)} %copy.152), calls=%async_computation.5 | async-start | bytes 524288 | tf_op jit(solution)/shard_map/all_to_all | solution.py:254
  188.5 12.8 %copy-start.14 = (f32[32,2,16,128]{3,2,1,0:T(8,128)}, f32[32,2,16,128]{3,2,1,0:T(8,128)S(1)}, u32[]{:S(2)}) copy-start(f32[32,2,16,128]{3,2,1,0:T(8,128)S(1)} %convert_element_type.117) | copy-start | bytes 1572868
  196.4 4.9 %copy-start.15 = (f32[32,2,16,128]{3,2,1,0:T(8,128)}, f32[32,2,16,128]{3,2,1,0:T(8,128)S(1)}, u32[]{:S(2)}) copy-start(f32[32,2,16,128]{3,2,1,0:T(8,128)S(1)} %convert_element_type.124) | copy-start | bytes 1572868
  196.4 53.9 %copy-start.22 = (f32[2,256,128]{2,1,0:T(8,128)S(1)}, f32[2,256,128]{2,1,0:T(8,128)}, u32[]{:S(2)}) copy-start(f32[2,256,128]{2,1,0:T(8,128)} %get-tuple-element.132) | copy-start | bytes 786436
  244.7 13.4 %all-to-all-start.4 = ((bf16[32,2,16,128]{3,2,1,0:T(8,128)(2,1)}), bf16[32,2,16,128]{3,2,1,0:T(8,128)(2,1)S(1)}, u32[]{:S(2)}, u32[]{:S(2)}) async-start(bf16[32,2,16,128]{3,2,1,0:T(8,128)(2,1)} %constant_dynamic-update-slice_fusion.32), calls=%async_computation.6 | async-start | bytes 524288 | tf_op jit(solution)/shard_map/all_to_all | solution.py:254
  252.5 22.6 %copy-start.29 = (bf16[192,2,128]{2,0,1:T(8,128)(2,1)S(1)}, bf16[192,2,128]{2,0,1:T(8,128)(2,1)}, u32[]{:S(2)}) copy-start(bf16[192,2,128]{2,0,1:T(8,128)(2,1)} %copy-done.28) | copy-start | bytes 294916
  258.1 13.4 %all-to-all-start.2 = ((bf16[32,2,16,128]{3,2,1,0:T(8,128)(2,1)}), bf16[32,2,16,128]{3,2,1,0:T(8,128)(2,1)}, u32[]{:S(2)}, u32[]{:S(2)}) async-start(bf16[32,2,16,128]{3,2,1,0:T(8,128)(2,1)} %constant_dynamic-update-slice_fusion), calls=%async_computation.4 | async-start | bytes 524288 | tf_op jit(solution)/shard_map/all_to_all | solution.py:254
  262.5 13.6 %copy-start.17 = (bf16[192,256]{1,0:T(8,128)(2,1)S(1)}, bf16[192,256]{1,0:T(8,128)(2,1)}, u32[]{:S(2)}) copy-start(bf16[192,256]{1,0:T(8,128)(2,1)} %param.13) | copy-start | bytes 294916
  262.6 8.9 %copy-start.18 = (f32[1,32,16,128]{3,2,1,0:T(8,128)}, f32[1,32,16,128]{3,2,1,0:T(8,128)S(1)}, u32[]{:S(2)}) copy-start(f32[1,32,16,128]{3,2,1,0:T(8,128)S(1)} %get-tuple-element.75) | copy-start | bytes 786436
  272.4 9.7 %copy-start.13 = (bf16[192,512]{1,0:T(8,128)(2,1)S(1)}, bf16[192,512]{1,0:T(8,128)(2,1)}, u32[]{:S(2)}) copy-start(bf16[192,512]{1,0:T(8,128)(2,1)} %param.15) | copy-start | bytes 589828
  276.1 7.3 %copy-start.37 = (f32[1,256]{1,0:T(1,128)S(1)}, f32[1,256]{1,0:T(1,128)}, u32[]{:S(2)}) copy-start(f32[1,256]{1,0:T(1,128)} %copy-done.36) | copy-start | bytes 3076
  282.1 3.7 %copy-start.19 = (f32[1,32,16,128]{3,2,1,0:T(8,128)S(1)}, f32[1,32,16,128]{3,2,1,0:T(8,128)}, u32[]{:S(2)}) copy-start(f32[1,32,16,128]{3,2,1,0:T(8,128)} %get-tuple-element.73) | copy-start | bytes 786436
  282.1 3.7 %copy-start.35 = (f32[192,2,128]{2,0,1:T(8,128)S(1)}, f32[192,2,128]{2,0,1:T(8,128)}, u32[]{:S(2)}) copy-start(f32[192,2,128]{2,0,1:T(8,128)} %fusion.19) | copy-start | bytes 589828
  282.1 5.3 %copy-start.21 = (f32[2,256,128]{1,2,0:T(8,128)S(1)}, f32[2,256,128]{1,2,0:T(8,128)}, u32[]{:S(2)}) copy-start(f32[2,256,128]{1,2,0:T(8,128)} %get-tuple-element.134) | copy-start | bytes 786436
  282.1 5.3 %copy-start.23 = (f32[2,256,128]{1,2,0:T(8,128)S(1)}, f32[2,256,128]{1,2,0:T(8,128)}, u32[]{:S(2)}) copy-start(f32[2,256,128]{1,2,0:T(8,128)} %copy.172) | copy-start | bytes 786436
  282.1 5.3 %copy-start.24 = (f32[2,256,128]{1,2,0:T(8,128)S(1)}, f32[2,256,128]{1,2,0:T(8,128)}, u32[]{:S(2)}) copy-start(f32[2,256,128]{1,2,0:T(8,128)} %copy.173) | copy-start | bytes 786436
  282.1 5.3 %copy-start.25 = (f32[2,256,128]{1,2,0:T(8,128)S(1)}, f32[2,256,128]{1,2,0:T(8,128)}, u32[]{:S(2)}) copy-start(f32[2,256,128]{1,2,0:T(8,128)} %copy.170) | copy-start | bytes 786436
  282.1 5.3 %copy-start.26 = (f32[2,256,128]{1,2,0:T(8,128)S(1)}, f32[2,256,128]{1,2,0:T(8,128)}, u32[]{:S(2)}) copy-start(f32[2,256,128]{1,2,0:T(8,128)} %copy.171) | copy-start | bytes 786436
  282.1 5.3 %copy-start.27 = (f32[2,256,128]{1,2,0:T(8,128)S(1)}, f32[2,256,128]{1,2,0:T(8,128)}, u32[]{:S(2)}) copy-start(f32[2,256,128]{1,2,0:T(8,128)} %copy.169) | copy-start | bytes 786436
  282.1 5.3 %copy-start.44 = (f32[2,128]{1,0:T(2,128)S(1)}, f32[2,128]{1,0:T(2,128)}, u32[]{:S(2)}) copy-start(f32[2,128]{1,0:T(2,128)} %get-tuple-element.115) | copy-start | bytes 3076
  (6 other events, 4.5 us)
Sparse Core Ops, SparseCore 0:
  77.2 37.1 reduce-scatter.2
  179.0 83.4 reduce-scatter.4
where the time goes:
time: 300 us; the launch traced here: 295 us
  Pallas kernels  75.3 us (25%)
  other arithmetic  56.4 us (19%)
  blocking collectives  37.1 us (12%)
  waiting for transfers between devices  31.6 us (11%)
  matrix products  28.3 us (9%)
  local copies, waits for them, and re-layouts  28.2 us (9%)
  starting transfers between devices  24 us (8%)
  between operations  14.7 us (5%)
    pallas_call x1, Pallas kernels, dispatch(): pl.pallas_call(dispatch_kernel, name='dispatch', out_shape=jax.ShapeDtype...  49.3 us
    unnamed x45, other arithmetic  48.9 us
    all_gather x1, blocking collectives, body(): decay = lax.all_gather(jnp.exp(total), 'sp')  24.8 us
    all_to_all x4, waiting for transfers between devices, exchange(): return lax.all_to_all(x, 'sp', split_axis=0, concat_axis=0, tiled=True)  21.3 us
    dot_general x17, matrix products, mm(): jnp.einsum(eq, a.astype(BF16), b.astype(BF16), preferred_element_type=F32)  20.3 us
    all_to_all x4, starting transfers between devices, exchange(): return lax.all_to_all(x, 'sp', split_axis=0, concat_axis=0, tiled=True)  19.6 us
    pallas_call x1, Pallas kernels, weight_grads(): pl.pallas_call(weight_grad_kernel, name='weight_grads', grid=(TP, 2), out...  12.7 us
    all_gather x1, blocking collectives, body(): token_grad = lax.all_gather(token_part, 'tp', axis=1, tiled=True)  12.3 us
  transfers between devices with their start and end apart: 7, of which 5 were waited for; matrix products, arithmetic and copies ran while one was open for 32% of the time, Pallas kernels for 4%

commit v1 on v0

--- a/solution.py
+++ b/solution.py
@@ -38,6 +38,13 @@
     return lax.dot_general(a, b, (dims, ((), ())), preferred_element_type=F32, precision=precision)
 
 
+def lower_mask():
+    row = lax.broadcasted_iota(jnp.int32, (TOK, TOK), 0)
+    return row >= lax.broadcasted_iota(jnp.int32, (TOK, TOK), 1)
+
+
+SIGMA = DK ** (-0.5)
+RISE, FALL, HEAD, TAIL = 0, 1, 2, 3
 NN = ((1,), (0,))
 NT = ((1,), (1,))
 TN = ((0,), (0,))
@@ -91,7 +98,11 @@
     )(routes_t, weight_t, rows, cot)
 
 
-def dispatch_kernel(send_ref, out_ref, ssem, rsem, fsem, gsem, lsem):
+def dispatch_kernel(
+    send_ref, q_ref, k_ref, v_ref, decay_ref,
+    out_ref, scale_ref, scaled_ref, score_ref, kv_ref, kvb_ref, total_ref,
+    ssem, rsem, fsem, gsem, lsem,
+):
     me, mx = lax.axis_index("sp"), lax.axis_index("tp")
     quarters = (mx, lax.rem(mx + 2, TP))
     sides = (lax.rem(mx + 1, TP), lax.rem(mx + 3, TP))
@@ -131,6 +142,30 @@
     own[0].wait()
     for way in range(2):
         forward(way, len(OFFS), me).start()
+
+    lower = lower_mask()
+    cum = dot(jnp.where(lower, 1.0, 0.0), decay_ref[...], NN, lax.Precision.HIGHEST)
+    total = cum[TOK - 1 : TOK]
+    for h in range(2):
+        total_ref[h] = jnp.broadcast_to(jnp.exp(total[:, h * DK : (h + 1) * DK]), (8, DK))
+    scales = (
+        jnp.exp(cum - 0.5 * total), jnp.exp(0.5 * total - cum), jnp.exp(cum), jnp.exp(total - cum)
+    )
+    for i, scale in enumerate(scales):
+        scale_ref[i] = scale
+        scaled_ref[0, i] = (q_ref[...].astype(F32) * scale).astype(BF16)
+        scaled_ref[1, i] = (k_ref[...].astype(F32) * scale).astype(BF16)
+    for h in range(2):
+        c = pl.ds(h * DK, DK)
+        v = v_ref[:, pl.ds(h * DV, DV)]
+        fwd = dot(scaled_ref[0, RISE, :, c], scaled_ref[1, FALL, :, c], NT)
+        bwd = dot(scaled_ref[0, FALL, :, c], scaled_ref[1, RISE, :, c], NT)
+        score_ref[h] = (jnp.where(lower, fwd, bwd) * SIGMA).astype(BF16)
+        for i, kind in enumerate((TAIL, HEAD)):
+            kv = dot(v, scaled_ref[1, kind, :, c], TN)
+            kv_ref[i, h] = kv
+            kvb_ref[i, pl.ds(h * DV, DV)] = kv.astype(BF16)
+
     for i, off in enumerate(OFFS):
         plane(0, i).wait_recv()
         for way in range(2):
@@ -147,14 +182,22 @@
             forward(way, i, src).wait()
 
 
-def dispatch(send):
+def dispatch(send, q, k, v, decay):
     n = len(OFFS)
     return pl.pallas_call(
         dispatch_kernel,
         name="dispatch",
-        out_shape=jax.ShapeDtypeStruct((2, TP, 3, SP, 8, QW), BF16),
-        in_specs=[pl.BlockSpec(memory_space=VM)],
-        out_specs=pl.BlockSpec(memory_space=VM),
+        out_shape=(
+            jax.ShapeDtypeStruct((2, TP, 3, SP, 8, QW), BF16),
+            jax.ShapeDtypeStruct((4, TOK, 2 * DK), F32),
+            jax.ShapeDtypeStruct((2, 4, TOK, 2 * DK), BF16),
+            jax.ShapeDtypeStruct((2, TOK, TOK), BF16),
+            jax.ShapeDtypeStruct((2, 2, DV, DK), F32),
+            jax.ShapeDtypeStruct((2, 2 * DV, DK), BF16),
+            jax.ShapeDtypeStruct((2, 8, DK), F32),
+        ),
+        in_specs=[pl.BlockSpec(memory_space=VM)] * 5,
+        out_specs=(pl.BlockSpec(memory_space=VM),) * 7,
         scratch_shapes=[
             pltpu.SemaphoreType.DMA((2, n)),
             pltpu.SemaphoreType.DMA((2, n)),
@@ -163,9 +206,9 @@
             pltpu.SemaphoreType.DMA((2,)),
         ],
         compiler_params=pltpu.CompilerParams(
-            collective_id=1, has_side_effects=True, vmem_limit_bytes=24 << 20
-        ),
-    )(send)
+            collective_id=1, has_side_effects=True, vmem_limit_bytes=32 << 20
+        ),
+    )(send, q, k, v, decay)
 
 
 def expert_kernel(rows_ref, gate_ref, up_ref, down_ref, part_ref, act_ref, dg_ref, du_ref):
@@ -246,94 +289,363 @@
     )(rows, act, dg, du)
 
 
-def heads(x, width):
-    return x.reshape(x.shape[0], 2, width)
-
-
-def exchange(x):
-    return lax.all_to_all(x, "sp", split_axis=0, concat_axis=0, tiled=True)
-
-
-def scan_states(decay, first, second, backward):
-    n = first.shape[1] * 2 // SP
-    both = jnp.stack([first, second], axis=0).reshape(2, SP, n, DK).transpose(1, 0, 2, 3)
-    got = exchange(both.astype(BF16)).astype(F32)
-    head = lax.axis_index("sp") // (SP // 2)
-    d = lax.dynamic_index_in_dim(decay, head, 1, keepdims=False)
-    acc = jnp.zeros_like(got[0])
-    outs = [None] * SP
-    for s in (range(SP - 1, -1, -1) if backward else range(SP)):
-        outs[s] = acc
-        acc = d[s][None, None, :] * acc + got[s]
-    back = exchange(jnp.stack(outs).astype(BF16)).astype(F32)
-    back = back.transpose(1, 0, 2, 3).reshape(2, 2, DV, DK)
-    return back[0], back[1]
+def give_back_kernel(
+    part_ref, place_ref, cot_ref, kvb_ref, total_ref,
+    tg_ref, carry_ref, decs_ref,
+    side_ref, sum_ref, back_ref, half_ref, half_got_ref, first_ref, second_ref,
+    xs, xr, ps, pr, ks, kr, ds_, dr, cs, cr, hs, hr, ts, tr, lsem,
+):
+    me, mx = lax.axis_index("sp"), lax.axis_index("tp")
+    n = len(OFFS)
+    xs_dev = tuple(lax.rem(mx + d, TP) for d in (1, 3))
+    across = lax.rem(mx + 2, TP)
+    barrier = pltpu.get_barrier_semaphore()
+    for off in OFFS:
+        pl.semaphore_signal(barrier, inc=1, device_id={"sp": moved(me, off, 1)})
+    for d in (1, 2, 3):
+        pl.semaphore_signal(barrier, inc=1, device_id={"tp": lax.rem(mx + d, TP)})
+    pl.semaphore_wait(barrier, n + 3)
+
+    def peer(i):
+        return me if i == n else moved(me, OFFS[i], 1)
+
+    def states_out(i):
+        to = peer(i)
+        return (
+            pltpu.make_async_remote_copy(
+                src_ref=kvb_ref.at[:, to], dst_ref=first_ref.at[me],
+                send_sem=ks.at[i], recv_sem=kr.at[i], device_id={"sp": to},
+            ),
+            pltpu.make_async_remote_copy(
+                src_ref=total_ref.at[to // (SP // 2)], dst_ref=decs_ref.at[me],
+                send_sem=ds_.at[i], recv_sem=dr.at[i], device_id={"sp": to},
+            ),
+        )
+
+    def states_back(i):
+        to = peer(i)
+        return pltpu.make_async_remote_copy(
+            src_ref=second_ref.at[to], dst_ref=carry_ref.at[:, me],
+            send_sem=cs.at[i], recv_sem=cr.at[i], device_id={"sp": to},
+        )
+
+    def aside(way, i):
+        to = peer(i)
+        return pltpu.make_async_remote_copy(
+            src_ref=part_ref.at[xs_dev[way], :, to], dst_ref=side_ref.at[way, :, to],
+            send_sem=xs.at[way, i], recv_sem=xr.at[way, i], device_id={"tp": xs_dev[way]},
+        )
+
+    def plane(half, i):
+        to = peer(i)
+        src = sum_ref.at[:, to] if half == 0 else part_ref.at[across, :, to]
+        return pltpu.make_async_remote_copy(
+            src_ref=src, dst_ref=back_ref.at[half, :, me],
+            send_sem=ps.at[half, i], recv_sem=pr.at[half, i], device_id={"sp": to},
+        )
+
+    own = (
+        pltpu.make_async_copy(kvb_ref.at[:, me], first_ref.at[me], lsem.at[0]),
+        pltpu.make_async_copy(total_ref.at[me // (SP // 2)], decs_ref.at[me], lsem.at[1]),
+        pltpu.make_async_copy(part_ref.at[across, :, me], back_ref.at[1, :, me], lsem.at[2]),
+    )
+    for copy in own:
+        copy.start()
+    for i in range(n):
+        for copy in states_out(i):
+            copy.start()
+    for i in range(n + 1):
+        for way in range(2):
+            aside(way, i).start()
+    for i in range(n):
+        plane(1, i).start()
+
+    own[0].wait()
+    own[1].wait()
+    for i in range(n):
+        for copy in states_out(i):
+            copy.wait()
+    scan_into(first_ref, decs_ref, second_ref)
+    for i in range(n):
+        states_back(i).start()
+    carry_ref[:, me] = second_ref[me]
+
+    for i in range(n + 1):
+        for way in range(2):
+            aside(way, i).wait()
+        to = peer(i)
+        total = (
+            part_ref[mx, :, to].astype(F32)
+            + side_ref[0, :, to].astype(F32) + side_ref[1, :, to].astype(F32)
+        ).astype(BF16)
+        if i < n:
+            sum_ref[:, to] = total
+            if i > 0:
+                plane(0, i - 1).start()
+        else:
+            plane(0, n - 1).start()
+            back_ref[0, :, me] = total
+
+    own[2].wait()
+    for i in range(n):
+        plane(1, i).wait()
+    place = place_ref[...]
+    half_ref[...] = dot(place, back_ref[1].reshape(24 * SP, QW), TN).astype(BF16)
+    over = pltpu.make_async_remote_copy(
+        src_ref=half_ref, dst_ref=half_got_ref, send_sem=hs, recv_sem=hr, device_id={"tp": across}
+    )
+    for i in range(n):
+        states_back(i).wait()
+    over.start()
+    for i in range(n):
+        plane(0, i).wait()
+    cols = pl.ds(pl.multiple_of(mx * QW, QW), QW)
+    token = cot_ref[:, cols].astype(F32) + dot(place, back_ref[0].reshape(24 * SP, QW), TN)
+    over.wait()
+    tg_ref[mx] = (token + half_got_ref[...].astype(F32)).astype(BF16)
+    spread = [
+        pltpu.make_async_remote_copy(
+            src_ref=tg_ref.at[mx], dst_ref=tg_ref.at[mx],
+            send_sem=ts.at[d], recv_sem=tr.at[d], device_id={"tp": lax.rem(mx + d + 1, TP)},
+        )
+        for d in range(3)
+    ]
+    for copy in spread:
+        copy.start()
+    for copy in spread:
+        copy.wait()
+
+
+def scan_into(got_ref, decs_ref, out_ref):
+    for state, order in ((0, range(SP)), (1, range(SP - 1, -1, -1))):
+        acc = jnp.zeros((16, DK), F32)
+        for s in order:
+            out_ref[s, state] = acc.astype(BF16)
+            acc = decs_ref[s, 0:1] * acc + got_ref[s, state].astype(F32)
+
+
+def give_back(part, place, cot, kvb, total):
+    n = len(OFFS)
+    dma = pltpu.SemaphoreType.DMA
+    return pl.pallas_call(
+        give_back_kernel,
+        name="give_back",
+        out_shape=(
+            jax.ShapeDtypeStruct((TP, TOK, QW), BF16),
+            jax.ShapeDtypeStruct((2, SP, 16, DK), BF16),
+            jax.ShapeDtypeStruct((SP, 8, DK), F32),
+        ),
+        in_specs=[pl.BlockSpec(memory_space=VM)] * 5,
+        out_specs=(pl.BlockSpec(memory_space=VM),) * 3,
+        scratch_shapes=[
+            VM((2, 3, SP, 8, QW), BF16),
+            VM((3, SP, 8, QW), BF16),
+            VM((2, 3, SP, 8, QW), BF16),
+            VM((TOK, QW), BF16),
+            VM((TOK, QW), BF16),
+            VM((SP, 2, 16, DK), BF16),
+            VM((SP, 2, 16, DK), BF16),
+            dma((2, n + 1)), dma((2, n + 1)), dma((2, n)), dma((2, n)),
+            dma((n,)), dma((n,)), dma((n,)), dma((n,)), dma((n,)), dma((n,)),
+            dma, dma, dma((3,)), dma((3,)), dma((3,)),
+        ],
+        compiler_params=pltpu.CompilerParams(
+            collective_id=2, has_side_effects=True, vmem_limit_bytes=32 << 20
+        ),
+    )(part, place, cot, kvb, total)
+
+
+def attention_kernel(
+    tg_ref, proj_ref, mixed_ref, q_ref, k_ref, v_ref,
+    scale_ref, scaled_ref, score_ref, kv_ref, kvc_ref, total_ref, decs_ref,
+    gp_ref, gq_ref, gk_ref, gv_ref, gd_ref,
+    gf_ref, qo_ref, qob_ref, first_ref, second_ref, carry_ref, local_ref,
+    keep_ref, give_ref, got_ref, share_ref, gather_ref,
+    qs, qr, cs, cr, ms, mr, gs, gr, lsem,
+):
+    me = lax.axis_index("sp")
+    n = len(OFFS)
+    core = lax.rem(me, 2)
+    chip = me // 2
+    barrier = pltpu.get_barrier_semaphore()
+    for off in OFFS:
+        pl.semaphore_signal(barrier, inc=1, device_id={"sp": moved(me, off, 1)})
+
+    def peer(i):
+        return moved(me, OFFS[i], 1)
+
+    def states_out(i):
+        to = peer(i)
+        return pltpu.make_async_remote_copy(
+            src_ref=qob_ref.at[:, to], dst_ref=first_ref.at[me],
+            send_sem=qs.at[i], recv_sem=qr.at[i], device_id={"sp": to},
+        )
+
+    def states_back(i):
+        to = peer(i)
+        return pltpu.make_async_remote_copy(
+            src_ref=second_ref.at[to], dst_ref=carry_ref.at[:, me],
+            send_sem=cs.at[i], recv_sem=cr.at[i], device_id={"sp": to},
+        )
+
+    chips = [i for i, off in enumerate(OFFS) if off[2] == 0]
+
+    def share(j):
+        to = peer(chips[j])
+        return pltpu.make_async_remote_copy(
+            src_ref=share_ref.at[to // 2], dst_ref=gather_ref.at[chip],
+            send_sem=gs.at[j], recv_sem=gr.at[j], device_id={"sp": to},
+        )
+
+    grad = None
+    for p in range(TP):
+        term = dot(tg_ref[p], proj_ref[:, pl.ds(p * QW, QW)], NT)
+        grad = term if grad is None else grad + term
+    gf_ref[...] = grad.astype(BF16)
+    for h in range(2):
+        gf = gf_ref[:, pl.ds(h * DV, DV)]
+        c = pl.ds(h * DK, DK)
+        for i, kind in enumerate((TAIL, HEAD)):
+            qo = dot(gf, scaled_ref[0, kind, :, c], TN)
+            qo_ref[i, h] = qo
+            qob_ref[i, pl.ds(h * SP // 2, SP // 2)] = qo.astype(BF16).reshape(SP // 2, 16, DK)
+    pl.semaphore_wait(barrier, n)
+    for i in range(n):
+        states_out(i).start()
+    first_ref[me] = qob_ref[:, me]
+
+    mixed = mixed_ref[...]
+    for p in range(TP):
+        part = dot(tg_ref[p], mixed, TN).reshape(4, 2, 64, QW)
+        for b in range(4):
+            keep_ref[p * 4 + b] = jnp.where(core == 0, part[b, 0], part[b, 1])
+            give_ref[p * 4 + b] = jnp.where(core == 0, part[b, 1], part[b, 0]).astype(BF16)
+    swap = pltpu.make_async_remote_copy(
+        src_ref=give_ref, dst_ref=got_ref, send_sem=ms, recv_sem=mr, device_id={"sp": peer(0)}
+    )
+    swap.start()
+
+    lower = lower_mask()
+    for h in range(2):
+        c = pl.ds(h * DK, DK)
+        gf, v = gf_ref[:, pl.ds(h * DV, DV)], v_ref[:, pl.ds(h * DV, DV)]
+        pair = dot(gf, v, NT)
+        fwd, bwd = jnp.where(lower, pair, 0.0).astype(BF16), jnp.where(lower, 0.0, pair).astype(BF16)
+        rise, fall = scale_ref[RISE, :, c], scale_ref[FALL, :, c]
+        local_ref[0, :, c] = rise * dot(fwd, scaled_ref[1, FALL, :, c], NN)
+        local_ref[1, :, c] = fall * dot(bwd, scaled_ref[1, RISE, :, c], NN)
+        local_ref[2, :, c] = fall * dot(fwd, scaled_ref[0, RISE, :, c], TN)
+        local_ref[3, :, c] = rise * dot(bwd, scaled_ref[0, FALL, :, c], TN)
+        gv_ref[:, pl.ds(h * DV, DV)] = dot(score_ref[h], gf, TN)
+
+    for i in range(n):
+        states_out(i).wait()
+    scan_into(first_ref, decs_ref, second_ref)
+    for i in range(n):
+        states_back(i).start()
+    carry_ref[:, me] = second_ref[me]
+    swap.wait()
+    for m in range(SP // 2):
+        share_ref[m] = (keep_ref[m] + got_ref[m].astype(F32)).astype(BF16)
+    for i in range(n):
+        states_back(i).wait()
+    for j in range(len(chips)):
+        share(j).start()
+
+    for h in range(2):
+        c = pl.ds(h * DK, DK)
+        rows = pl.ds(h * SP // 2, SP // 2)
+        vcols = pl.ds(h * DV, DV)
+        gf, v = gf_ref[:, vcols], v_ref[:, vcols]
+        qo_low, qo_high = carry_ref[0, rows].reshape(DV, DK), carry_ref[1, rows].reshape(DV, DK)
+        kv_low, kv_high = kvc_ref[0, rows].reshape(DV, DK), kvc_ref[1, rows].reshape(DV, DK)
+        head, tail = scale_ref[HEAD, :, c], scale_ref[TAIL, :, c]
+        q_fwd = local_ref[0, :, c] + head * dot(gf, kv_low, NN)
+        q_bwd = local_ref[1, :, c] + tail * dot(gf, kv_high, NN)
+        k_fwd = local_ref[2, :, c] + tail * dot(v, qo_high, NN)
+        k_bwd = local_ref[3, :, c] + head * dot(v, qo_low, NN)
+        gq_ref[:, c] = SIGMA * (q_fwd + q_bwd)
+        gk_ref[:, c] = SIGMA * (k_fwd + k_bwd)
+        gv_ref[:, vcols] = gv_ref[:, vcols] + SIGMA * (
+            dot(scaled_ref[1, TAIL, :, c], qo_high, NT) + dot(scaled_ref[1, HEAD, :, c], qo_low, NT)
+        )
+        grad_cum = SIGMA * (
+            q_ref[:, c].astype(F32) * (q_fwd - q_bwd) - k_ref[:, c].astype(F32) * (k_fwd - k_bwd)
+        )
+        decay = total_ref[h, 0:1]
+        beyond = SIGMA * jnp.sum(
+            (decay * kv_low.astype(F32) + kv_ref[0, h]) * qo_high.astype(F32)
+            + (decay * qo_low.astype(F32) + qo_ref[0, h]) * kv_high.astype(F32),
+            axis=0, keepdims=True,
+        )
+        upper = jnp.where(
+            lax.broadcasted_iota(jnp.int32, (TOK, TOK), 0)
+            <= lax.broadcasted_iota(jnp.int32, (TOK, TOK), 1), 1.0, 0.0,
+        )
+        gd_ref[:, c] = dot(upper, grad_cum, NN, lax.Precision.HIGHEST) + beyond
+
+    for j in range(len(chips)):
+        share(j).wait()
+    total = share_ref[chip].astype(F32)
+    for j in range(len(chips)):
+        dy, dz, _ = OFFS[chips[j]]
+        total = total + gather_ref[moved(me, (dy, dz, 0), -1) // 2].astype(F32)
+    gp_ref[...] = total
+
+
+def attention(*operands):
+    n = len(OFFS)
+    dma = pltpu.SemaphoreType.DMA
+    small = jax.ShapeDtypeStruct((TOK, 2 * DK), F32)
+    return pl.pallas_call(
+        attention_kernel,
+        name="attention",
+        out_shape=(
+            jax.ShapeDtypeStruct((64, QW), F32), small, small,
+            jax.ShapeDtypeStruct((TOK, 2 * DV), F32), small,
+        ),
+        in_specs=[pl.BlockSpec(memory_space=VM)] * len(operands),
+        out_specs=(pl.BlockSpec(memory_space=VM),) * 5,
+        scratch_shapes=[
+            VM((TOK, 2 * DV), BF16),
+            VM((2, 2, DV, DK), F32),
+            VM((2, SP, 16, DK), BF16),
+            VM((SP, 2, 16, DK), BF16),
+            VM((SP, 2, 16, DK), BF16),
+            VM((2, SP, 16, DK), BF16),
+            VM((4, TOK, 2 * DK), F32),
+            VM((SP // 2, 64, QW), F32),
+            VM((SP // 2, 64, QW), BF16),
+            VM((SP // 2, 64, QW), BF16),
+            VM((SP // 2, 64, QW), BF16),
+            VM((SP // 2, 64, QW), BF16),
+            dma((n,)), dma((n,)), dma((n,)), dma((n,)), dma, dma, dma((15,)), dma((15,)), dma,
+        ],
+        compiler_params=pltpu.CompilerParams(
+            collective_id=3, has_side_effects=True, vmem_limit_bytes=40 << 20
+        ),
+    )(*operands)
 
 
 def body(
     queries, key_vectors, values_in, log_decay, mixed_heads, out_proj, layer_input, cotangent,
     routes, route_weight, gate_weight, up_weight, down_weight,
 ):
-    mx = lax.axis_index("tp")
     place, send = prep(routes.T, route_weight.T, layer_input, cotangent)
-    got = dispatch(send.reshape(2, 2, 3, SP, 8, QW)).reshape(2, TP, 24 * SP, QW)
+    got, scale, scaled, score, kv, kvb, total = dispatch(
+        send.reshape(2, 2, 3, SP, 8, QW), queries, key_vectors, values_in, log_decay
+    )
+    got = got.reshape(2, TP, 24 * SP, QW)
     part, act, dg, du = experts(got, gate_weight, up_weight, down_weight)
+    tg, carry, decs = give_back(
+        part.reshape(TP, 3, SP, 8, QW), place, cotangent, kvb.reshape(2, SP, 16, DK), total
+    )
     grad_gate, grad_up, grad_down = weight_grads(got, act, dg, du)
-    mine = lax.psum_scatter(part, "tp", scatter_dimension=0, tiled=True)
-    back = lax.all_to_all(
-        mine.reshape(3, SP, 8, QW), "sp", split_axis=1, concat_axis=1, tiled=True
-    ).reshape(24 * SP, QW)
-    own_cot = lax.dynamic_slice_in_dim(cotangent, mx * QW, QW, 1)
-    token_part = (own_cot.astype(F32) + dot(place, back, TN)).astype(BF16)
-    token_grad = lax.all_gather(token_part, "tp", axis=1, tiled=True)
-    grad_proj = lax.psum_scatter(
-        dot(token_grad, mixed_heads, TN), "sp", scatter_dimension=0, tiled=True
-    )
-    sigma = DK ** (-0.5)
-    grad_f = heads(dot(token_grad, out_proj, NT), DV)
-    q, k, v = heads(queries, DK).astype(F32), heads(key_vectors, DK).astype(F32), heads(values_in, DV)
-    t_row = lax.broadcasted_iota(jnp.int32, (TOK, TOK), 0)
-    t_col = lax.broadcasted_iota(jnp.int32, (TOK, TOK), 1)
-    lower = t_row >= t_col
-    cum = heads(dot(lower.astype(F32), log_decay, NN, lax.Precision.HIGHEST), DK)
-    total = cum[-1]
-    rise, fall = jnp.exp(cum - 0.5 * total), jnp.exp(0.5 * total - cum)
-    head, tail = jnp.exp(cum), jnp.exp(total - cum)
-    decay = lax.all_gather(jnp.exp(total), "sp")
-
-    def mm(eq, a, b):
-        return jnp.einsum(eq, a.astype(BF16), b.astype(BF16), preferred_element_type=F32)
-
-    qr, qf, kr, kf = q * rise, q * fall, k * rise, k * fall
-    qh, qt, kh, kt = q * head, q * tail, k * head, k * tail
-    score = sigma * (
-        jnp.where(lower, mm("thc,shc->hts", qr, kf), 0.0) + jnp.where(lower, 0.0, mm("thc,shc->hts", qf, kr))
-    )
-    pair = mm("thv,shv->hts", grad_f, v)
-    pair_fwd, pair_bwd = jnp.where(lower, pair, 0.0), jnp.where(lower, 0.0, pair)
-    kv_fwd, kv_bwd = mm("shv,shc->hvc", v, kt), mm("shv,shc->hvc", v, kh)
-    qo_bwd, qo_fwd = mm("thv,thc->hvc", grad_f, qt), mm("thv,thc->hvc", grad_f, qh)
-    kv_low, qo_low = scan_states(decay, kv_fwd, qo_bwd, False)
-    qo_high, kv_high = scan_states(decay, qo_fwd, kv_bwd, True)
-    q_fwd = sigma * (rise * mm("hts,shc->thc", pair_fwd, kf) + head * mm("thv,hvc->thc", grad_f, kv_low))
-    q_bwd = sigma * (fall * mm("hts,shc->thc", pair_bwd, kr) + tail * mm("thv,hvc->thc", grad_f, kv_high))
-    k_fwd = sigma * (fall * mm("hts,thc->shc", pair_fwd, qr) + tail * mm("shv,hvc->shc", v, qo_high))
-    k_bwd = sigma * (rise * mm("hts,thc->shc", pair_bwd, qf) + head * mm("shv,hvc->shc", v, qo_low))
-    value_grad = mm("hts,thv->shv", score, grad_f) + sigma * (
-        mm("shc,hvc->shv", kt, qo_high) + mm("shc,hvc->shv", kh, qo_low)
-    )
-    grad_cum = (q * (q_fwd - q_bwd) - k * (k_fwd - k_bwd)).reshape(TOK, 2 * DK)
-    d_own = jnp.exp(total)[:, None, :]
-    beyond = sigma * jnp.sum(
-        (d_own * kv_low + kv_fwd) * qo_high + (d_own * qo_low + qo_bwd) * kv_high, axis=1
-    ).reshape(1, 2 * DK)
-    upper = (t_row <= t_col).astype(F32)
-    grad_decay = dot(upper, grad_cum, NN, lax.Precision.HIGHEST) + beyond
-    return (
-        grad_gate, grad_up, grad_down, grad_proj,
-        (q_fwd + q_bwd).reshape(TOK, 2 * DK), (k_fwd + k_bwd).reshape(TOK, 2 * DK),
-        value_grad.reshape(TOK, 2 * DV), grad_decay,
-    )
+    grad_proj, grad_q, grad_k, grad_v, grad_decay = attention(
+        tg, out_proj, mixed_heads, queries, key_vectors, values_in,
+        scale, scaled, score, kv, carry, total, decs,
+    )
+    return grad_gate, grad_up, grad_down, grad_proj, grad_q, grad_k, grad_v, grad_decay
 
 
 def solution(mesh):

time: 300 us -> 173 us (0.58); the launches traced: 295 us -> 173 us
  Pallas kernels: 75.3 us -> 157 us
  other arithmetic: 56.4 us -> 0 us
  blocking collectives: 37.1 us -> 0 us
  waiting for transfers between devices: 31.6 us -> 0 us
  matrix products: 28.3 us -> 0 us
  starting transfers between devices: 24 us -> 0 us
  between operations: 14.7 us -> 0.78 us
  local copies, waits for them, and re-layouts: 28.2 us -> 15.3 us
    pallas_call x1 -> x3, Pallas kernels: 49.3 us -> 131 us  [the longest x1 49.1 us: dispatch(): pl.pallas_call(dispatch_kernel, name='dispatch', out_shape=(jax.ShapeDtyp...]
    unnamed x45 -> x0, other arithmetic: 48.9 us -> none
    all_gather x2 -> x0, blocking collectives: 37.1 us -> none  [the longest x1 24.8 us: body(): decay = lax.all_gather(jnp.exp(total), 'sp')]
    all_to_all x5 -> x0, waiting for transfers between devices: 31.6 us -> none  [the longest x4 21.3 us: exchange(): return lax.all_to_all(x, 'sp', split_axis=0, concat_axis=0, tiled=True)]
    dot_general x22 -> x0, matrix products: 28.3 us -> none  [the longest x17 20.3 us: mm(): jnp.einsum(eq, a.astype(BF16), b.astype(BF16), preferred_element_type=F32)]
    all_to_all x5 -> x0, starting transfers between devices: 23.9 us -> none  [the longest x4 19.6 us: exchange(): return lax.all_to_all(x, 'sp', split_axis=0, concat_axis=0, tiled=True)]
    reshape x4 -> x0, local copies, waits for them, and re-layouts: 5.25 us -> none  [the longest x1 2.08 us: body(): mine.reshape(3, SP, 8, QW)]
    unnamed x96 -> x41, local copies, waits for them, and re-layouts: 10.9 us -> 15.3 us
  transfers between devices with their start and end apart: 7 -> 0, of which waited for: 5 -> 0; matrix products, arithmetic and copies ran while one was open for 32% -> 0% of each run, Pallas kernels for 4% -> 0%
where the time goes in v1:
time: 173 us
  Pallas kernels  157 us (91%)
  local copies, waits for them, and re-layouts  15.3 us (9%)
    pallas_call x1, Pallas kernels, dispatch(): pl.pallas_call(dispatch_kernel, name='dispatch', out_shape=(jax.ShapeDtyp...  49.1 us
    pallas_call x1, Pallas kernels, give_back(): pl.pallas_call(give_back_kernel, name='give_back', out_shape=(jax.ShapeDt...  47.9 us
    pallas_call x1, Pallas kernels, attention(): pl.pallas_call(attention_kernel, name='attention', out_shape=(jax.ShapeDt...  33.5 us
    unnamed x41, local copies, waits for them, and re-layouts  15.3 us
    pallas_call x1, Pallas kernels, weight_grads(): pl.pallas_call(weight_grad_kernel, name='weight_grads', grid=(TP, 2), out...  12.7 us
    pallas_call x1, Pallas kernels, experts(): pl.pallas_call(expert_kernel, name='experts', out_shape=(jax.ShapeDtypeSt...  12 us

profile of v1, /device:TPU:1, one launch (start us, length us, event | category | flops | bytes accessed | tf_op | source)
XLA Modules:
  0.0 172.6 jit_solution(7567060645112300629)
XLA Ops:
  0.6 0.0 copy-start.1
  0.6 1.1 copy-done.1
  1.8 0.0 copy-start.9
  1.8 1.1 copy-done.9
  2.9 0.0 copy-start.16
  2.9 0.7 copy-done.16
  3.6 0.0 copy-start.17
  3.6 0.7 copy-done.17
  4.3 0.0 copy-start.5
  4.3 0.0 copy-start.6
  4.3 1.3 prep.1
  5.5 0.0 copy-start.7
  5.5 0.9 copy-done.7
  6.5 0.0 copy-start.10
  6.5 0.9 copy-done.10
  7.4 0.0 copy-start.12
  7.4 0.9 copy-done.12
  8.2 0.0 copy-start.14
  8.2 0.9 copy-done.14
  9.2 49.1 %dispatch.1 = (bf16[2,4,3,32,8,512]{5,4,3,2,1,0:T(8,128)(2,1)S(1)}, f32[4,192,256]{2,1,0:T(8,128)S(1)}, bf16[2,4,192,256]{3,2,1,0:T(8,128)(2,1)S(1)}, bf16[2,192...) custom-call(bf16[2,2,3,32,8,512]{5,4,3,2,1,0:T(8,128)(2,1)S(1)} %bit, ...), custom_call_target="tpu_custom_call" | custom-call | tf_op jit(solution)/shard_map/dispatch/pallas_call | solution.py:187
  58.3 0.0 copy-start
  58.3 2.6 %copy-done = bf16[2,4,3,32,8,512]{5,4,3,2,1,0:T(8,128)(2,1)} copy-done((bf16[2,4,3,32,8,512]{5,4,3,2,1,0:T(8,128)(2,1)}, bf16[2,4,3,32,8,512]{5,4,3,2,1,0:T(8,128)(2,1)S(1)}, u32[]{:S(2)}) %copy-start) | copy-done | bytes 6291480
  61.0 0.0 copy-done.5
  61.0 0.0 copy-done.6
  61.0 0.0 copy-start.2
  61.0 0.0 copy-start.4
  61.0 0.0 copy-start.8
  61.0 0.0 copy-start.11
  61.0 0.0 copy-start.13
  61.0 0.0 copy-start.15
  61.0 12.0 %experts.1 = (bf16[4,768,512]{2,1,0:T(8,128)(2,1)}, bf16[2,512,256]{2,1,0:T(8,128)(2,1)S(1)}, bf16[2,512,256]{2,1,0:T(8,128)(2,1)S(1)}, bf16[2,512,256]{2,1,0:T(8,128)(2,1)S(1)}) custom-call(bf16[2,4,768,512]{3,2,1,0:T(8,128)(2,1)} %bitcast.6, bf16[2,2048,256]{2,1,0:T(8,128)(2,1)S(1)} %copy-done.5, bf16[2,2048,256]{2,1,0:T(8,128)(2,1)S(1)} %copy-done.6, ...), custom_call_target="tpu_custom_call" | custom-call | tf_op jit(solution)/shard_map/experts/pallas_call | solution.py:254
  73.1 0.0 copy-done.2
  73.1 0.0 copy-start.3
  73.1 1.9 %copy-done.3 = bf16[4,768,512]{2,1,0:T(8,128)(2,1)S(1)} copy-done((bf16[4,768,512]{2,1,0:T(8,128)(2,1)S(1)}, bf16[4,768,512]{2,1,0:T(8,128)(2,1)}, u32[]{:S(2)}) %copy-start.3) | copy-done | bytes 3145752
  75.0 47.9 %give_back.1 = (bf16[4,192,512]{2,1,0:T(8,128)(2,1)S(1)}, bf16[2,32,16,128]{3,2,1,0:T(8,128)(2,1)S(1)}, f32[32,8,128]{2,1,0:T(8,128)S(1)}) custom-call(bf16[4,3,32,8,512]{4,3,2,1,0:T(8,128)(2,1)S(1)} %bitcast.9, bf16[768,192]{1,0:T(8,128)(2,1)S(1)} %get-tuple-element.41.place_ref, bf16[192,2048]{1,0:T(8,128)(2,1)S(1)} %copy-done.2, ...), custom_call_target="tpu_custom_call" | custom-call | tf_op jit(solution)/shard_map/give_back/pallas_call | solution.py:430
  122.9 0.0 copy-done.4
  122.9 0.0 copy-done.8
  122.9 0.0 copy-done.11
  122.9 0.0 copy-done.13
  123.0 0.0 copy-done.15
  123.0 33.5 %attention.1 = (f32[64,512]{1,0:T(8,128)S(1)}, f32[192,256]{1,0:T(8,128)S(1)}, f32[192,256]{1,0:T(8,128)S(1)}, f32[192,512]{1,0:T(8,128)S(1)}, f32[192,256]{1,0:T(8,128)S(1)}) custom-call(bf16[4,192,512]{2,1,0:T(8,128)(2,1)S(1)} %get-tuple-element.44.tg_ref, bf16[512,2048]{1,0:T(8,128)(2,1)S(1)} %copy-done.4, bf16[192,512]{1,0:T(8,128)(2,1)S(1)} %copy-done.15, ...), custom_call_target="tpu_custom_call" | custom-call | tf_op jit(solution)/shard_map/attention/pallas_call | solution.py:600
  156.4 12.7 %weight_grads.1 = (f32[2,2048,256]{2,1,0:T(8,128)}, f32[2,2048,256]{2,1,0:T(8,128)}, f32[2,256,2048]{2,1,0:T(8,128)}) custom-call(bf16[2,4,768,512]{3,2,1,0:T(8,128)(2,1)} %bitcast.7, bf16[2,512,256]{2,1,0:T(8,128)(2,1)S(1)} %get-tuple-element.34.act_ref, bf16[2,512,256]{2,1,0:T(8,128)(2,1)S(1)} %get-tuple-element.35.dg_ref, ...), custom_call_target="tpu_custom_call" | custom-call | tf_op jit(solution)/shard_map/weight_grads/pallas_call | solution.py:275
  169.1 0.7 copy.26
  169.8 0.7 copy.27
  170.5 0.7 copy.28
  171.1 0.7 copy.29
  171.9 0.7 copy.30
Async XLA Ops:
  0.6 1.1 copy-start.1
  1.8 1.1 copy-start.9
  2.9 0.7 copy-start.16
  3.6 0.7 copy-start.17
  4.3 56.7 %copy-start.5 = (bf16[2,2048,256]{2,1,0:T(8,128)(2,1)S(1)}, bf16[2,2048,256]{2,1,0:T(8,128)(2,1)}, u32[]{:S(2)}) copy-start(bf16[2,2048,256]{2,1,0:T(8,128)(2,1)} %gate_ref.1) | copy-start | bytes 6291460
  4.3 56.7 %copy-start.6 = (bf16[2,2048,256]{2,1,0:T(8,128)(2,1)S(1)}, bf16[2,2048,256]{2,1,0:T(8,128)(2,1)}, u32[]{:S(2)}) copy-start(bf16[2,2048,256]{2,1,0:T(8,128)(2,1)} %up_ref.1) | copy-start | bytes 6291460
  5.5 0.9 copy-start.7
  6.5 0.9 copy-start.10
  7.4 0.9 copy-start.12
  8.2 0.9 copy-start.14
  58.3 2.7 %copy-start = (bf16[2,4,3,32,8,512]{5,4,3,2,1,0:T(8,128)(2,1)}, bf16[2,4,3,32,8,512]{5,4,3,2,1,0:T(8,128)(2,1)S(1)}, u32[]{:S(2)}) copy-start(bf16[2,4,3,32,8,512]{5,4,3,2,1,0:T(8,128)(2,1)S(1)} %get-tuple-element.33) | copy-start | bytes 18874372
  61.0 12.1 %copy-start.2 = (bf16[192,2048]{1,0:T(8,128)(2,1)S(1)}, bf16[192,2048]{1,0:T(8,128)(2,1)}, u32[]{:S(2)}) copy-start(bf16[192,2048]{1,0:T(8,128)(2,1)} %cot_ref.3) | copy-start | bytes 2359300
  61.0 61.9 %copy-start.4 = (bf16[512,2048]{1,0:T(8,128)(2,1)S(1)}, bf16[512,2048]{1,0:T(8,128)(2,1)}, u32[]{:S(2)}) copy-start(bf16[512,2048]{1,0:T(8,128)(2,1)} %proj_ref.1) | copy-start | bytes 6291460
  61.0 61.9 %copy-start.8 = (bf16[192,512]{1,0:T(8,128)(2,1)S(1)}, bf16[192,512]{1,0:T(8,128)(2,1)}, u32[]{:S(2)}) copy-start(bf16[192,512]{1,0:T(8,128)(2,1)} %v_ref.3) | copy-start | bytes 589828
  61.0 61.9 %copy-start.11 = (bf16[192,256]{1,0:T(8,128)(2,1)S(1)}, bf16[192,256]{1,0:T(8,128)(2,1)}, u32[]{:S(2)}) copy-start(bf16[192,256]{1,0:T(8,128)(2,1)} %q_ref.3) | copy-start | bytes 294916
  61.0 61.9 %copy-start.13 = (bf16[192,256]{1,0:T(8,128)(2,1)S(1)}, bf16[192,256]{1,0:T(8,128)(2,1)}, u32[]{:S(2)}) copy-start(bf16[192,256]{1,0:T(8,128)(2,1)} %k_ref.3) | copy-start | bytes 294916
  61.0 61.9 %copy-start.15 = (bf16[192,512]{1,0:T(8,128)(2,1)S(1)}, bf16[192,512]{1,0:T(8,128)(2,1)}, u32[]{:S(2)}) copy-start(bf16[192,512]{1,0:T(8,128)(2,1)} %mixed_ref.1) | copy-start | bytes 589828
  73.1 1.9 %copy-start.3 = (bf16[4,768,512]{2,1,0:T(8,128)(2,1)S(1)}, bf16[4,768,512]{2,1,0:T(8,128)(2,1)}, u32[]{:S(2)}) copy-start(bf16[4,768,512]{2,1,0:T(8,128)(2,1)} %get-tuple-element.40) | copy-start | bytes 9437188
